TPU v7x, 32 devices: a whole 2x2x4 slice. The times are simulated.
32 devices in a mesh: rep: 2 (over x), fs: 8 (over z, y), tp: 2 (over core).
Axes of the slice: x: 2, y: 2, z: 4, core: 2. Of those that a mesh axis runs over, the one named last changes fastest.
Arguments:
- tokens: bfloat16 [6144, 2048], P(('rep', 'fs'), 'tp'), may hold values from -6 to 6
- mix_gain: float32 [2048], replicated, may hold values from 0.1 to 1.9
- w_u: bfloat16 [2048, 2048], P('fs', 'tp'), may hold values from -0.125 to 0.125
- w_v: bfloat16 [2048, 2048], P('fs', 'tp'), may hold values from -0.125 to 0.125
- norm_gain: float32 [2048], P('tp'), may hold values from 0.1 to 1.9
- mix_weight: bfloat16 [16, 128, 128], P('tp'), may hold values from -0.5 to 0.5
- mix_bias: float32 [16, 128], P('tp'), may hold values from 0.1 to 1.9
- w_mix_out: bfloat16 [2048, 2048], P('tp', 'fs'), may hold values from -0.125 to 0.125
- ffn_gain: float32 [2048], replicated, may hold values from 0.1 to 1.9
- w_gate: bfloat16 [2048, 3072], P('fs', 'tp'), may hold values from -0.125 to 0.125
- w_value: bfloat16 [2048, 3072], P('fs', 'tp'), may hold values from -0.125 to 0.125
- taps_gate: bfloat16 [3, 3072], P(None, 'tp'), may hold values from -3.5 to 3.5
- taps_value: bfloat16 [3, 3072], P(None, 'tp'), may hold values from -3.5 to 3.5
- w_down: bfloat16 [3072, 2048], P('tp', 'fs'), may hold values from -0.109375 to 0.109375
Outputs:
- layer_out: bfloat16 [6144, 2048], P(('rep', 'fs'), 'tp')
All inputs are finite; a program needn't handle non-finite values.
Results may differ from a plain program's by a relative error of at most 0.017.
Values may be sent and summed in bfloat16 or wider, within the bound.
A program may use at most 64 MiB of HBM per device.

v0:
```python
import jax
import jax.numpy as jnp
from jax import lax
from jax.sharding import PartitionSpec as P

EPS_RMS = 1e-06
EPS_LN = 1e-05


def rms_scale(features, gain_vec):
    values = features.astype(jnp.float32)
    scaled = values * lax.rsqrt(jnp.mean(values * values, axis=-1, keepdims=True) + EPS_RMS)
    return (scaled * gain_vec).astype(jnp.bfloat16)


def spatial_mix(u_pre, v_pre, norm_gain, mix_weight, mix_bias):
    row_count = u_pre.shape[0]
    groups = mix_weight.shape[0]
    block_len = mix_weight.shape[1]
    group_width = v_pre.shape[1] // groups
    activated = jax.nn.gelu(v_pre).reshape(row_count, groups, group_width)
    average = jnp.mean(activated, axis=-1, keepdims=True)
    spread_sq = jnp.mean(jnp.square(activated - average), axis=-1, keepdims=True)
    v_norm = (
        (activated - average)
        * lax.rsqrt(spread_sq + EPS_LN)
        * norm_gain.reshape(groups, group_width)
    ).astype(jnp.bfloat16)
    blocks = v_norm.reshape(row_count // block_len, block_len, groups, group_width)
    lower_mask = jnp.arange(block_len)[:, None] >= jnp.arange(block_len)[None, :]
    masked = jnp.where(lower_mask[None], mix_weight, jnp.zeros_like(mix_weight))
    mixed_rows = jnp.einsum("gts,nsgc->ntgc", masked, blocks, preferred_element_type=jnp.float32)
    mixed_rows = mixed_rows + jnp.transpose(mix_bias)[None, :, :, None]
    mixed_rows = mixed_rows.reshape(row_count, groups * group_width)
    return (jax.nn.gelu(u_pre) * mixed_rows).astype(jnp.bfloat16)


def causal_taps(values, tap_weights):
    seq_len = values.shape[0]
    conv_len = tap_weights.shape[0]
    padded = jnp.pad(values, ((conv_len - 1, 0), (0, 0)))
    summed_terms = jnp.zeros_like(values)
    for tap_index in range(conv_len):
        summed_terms = (
            summed_terms
            + tap_weights[tap_index].astype(jnp.float32) * padded[tap_index : tap_index + seq_len]
        )
    return summed_terms


def add_pair(operand, pieces):
    first = jnp.dot(operand, pieces[0], preferred_element_type=jnp.float32)
    second = jnp.dot(operand, pieces[1], preferred_element_type=jnp.float32)
    return (first, second)


def project_with(operand, weight_piece):
    return jnp.dot(operand, weight_piece, preferred_element_type=jnp.float32)


def on_device(
    tokens,
    mix_gain,
    w_u,
    w_v,
    norm_gain,
    mix_weight,
    mix_bias,
    w_mix_out,
    ffn_gain,
    w_gate,
    w_value,
    taps_gate,
    taps_value,
    w_down,
):
    own_width = tokens.shape[1]
    features = lax.all_gather(tokens, "tp", axis=1, tiled=True)
    normed = rms_scale(features, mix_gain)
    u_pre, v_pre = add_pair(
        normed,
        (
            lax.all_gather(w_u, "fs", axis=0, tiled=True),
            lax.all_gather(w_v, "fs", axis=0, tiled=True),
        ),
    )
    hidden = spatial_mix(u_pre, v_pre, norm_gain, mix_weight, mix_bias)
    mixer_terms = project_with(hidden, lax.all_gather(w_mix_out, "fs", axis=1, tiled=True))
    mixer_full = lax.psum(mixer_terms.astype(jnp.bfloat16), "tp").astype(jnp.float32)
    middle = (features.astype(jnp.float32) + mixer_full).astype(jnp.bfloat16)
    middle_own = lax.dynamic_slice_in_dim(middle, lax.axis_index("tp") * own_width, own_width, 1)
    normed_mid = rms_scale(middle, ffn_gain)
    gate_pre, value_pre = add_pair(
        normed_mid,
        (
            lax.all_gather(w_gate, "fs", axis=0, tiled=True),
            lax.all_gather(w_value, "fs", axis=0, tiled=True),
        ),
    )
    activation = (
        jax.nn.gelu(causal_taps(gate_pre, taps_gate)) * causal_taps(value_pre, taps_value)
    ).astype(jnp.bfloat16)
    down_terms = project_with(activation, lax.all_gather(w_down, "fs", axis=1, tiled=True))
    channel_part = lax.psum_scatter(
        down_terms.astype(jnp.bfloat16), "tp", scatter_dimension=1, tiled=True
    ).astype(jnp.float32)
    return (middle_own.astype(jnp.float32) + channel_part).astype(jnp.bfloat16)


def solution(mesh):
    placed = (
        P(("rep", "fs"), "tp"),
        P(),
        P("fs", "tp"),
        P("fs", "tp"),
        P("tp"),
        P("tp", None, None),
        P("tp", None),
        P("tp", "fs"),
        P(),
        P("fs", "tp"),
        P("fs", "tp"),
        P(None, "tp"),
        P(None, "tp"),
        P("tp", "fs"),
    )
    return jax.shard_map(
        on_device, mesh=mesh, in_specs=placed, out_specs=P(("rep", "fs"), "tp"), check_vma=False
    )
```

profile of v0, /device:TPU:0, one launch (start us, length us, event | category | flops | bytes accessed | tf_op | source)
XLA Modules:
  0.0 603.2 jit_solution(8310468312568662907)
XLA Ops:
  6.5 0.0 copy-start.6
  6.5 0.0 all-gather.8.cloned.1.call-start
  6.5 0.7 all-gather.8.cloned.1.call-update
  7.3 0.0 all-gather.12.cloned.1.call-start
  7.3 0.7 all-gather.12.cloned.1.call-update
  8.0 0.0 all-gather.10.cloned.1.call-start
  8.1 0.7 all-gather.10.cloned.1.call-update
  8.7 0.0 all-gather.14.cloned.1.call-start
  8.8 0.5 all-gather.14.cloned.1.call-update
  9.3 0.0 all-reduce.4.cloned.1.call-start
  9.4 12.0 %all-gather.8.cloned.1.call-done = bf16[384,2048]{1,0:T(8,128)(2,1)} async-done(((bf16[384,1024]{1,0:T(8,128)(2,1)}), bf16[384,2048]{1,0:T(8,128)(2,1)}) %all-gather.8.cloned.1.call-update) | async-done | bytes 1572880 | tf_op jit(solution)/shard_map/all_gather | solution.py:78
  21.4 1.8 fusion.3
  23.2 74.3 %all-gather.12.cloned.1.call-done = bf16[2048,1024]{1,0:T(8,128)(2,1)} async-done(((bf16[256,1024]{1,0:T(8,128)(2,1)}), bf16[2048,1024]{1,0:T(8,128)(2,1)}) %all-gather.12.cloned.1.call-update) | async-done | bytes 4194320 | tf_op jit(solution)/shard_map/all_gather | solution.py:84
  97.6 0.0 copy-done.6
  97.6 4.8 fusion.32
  102.3 0.3 copy.38
  102.7 0.5 reduce_sum.37
  103.2 0.1 copy.30
  103.3 0.2 copy.33
  103.4 0.0 copy-start.1
  103.4 0.0 copy-start.4
  103.4 0.0 copy-start.5
  103.5 0.9 multiply_reduce_fusion
  104.4 0.1 copy.34
  104.5 0.6 copy.32
  105.0 0.0 copy-done.1
  105.1 0.0 copy-done.4
  105.1 0.0 copy-done.5
  105.1 0.4 bitcast_add_fusion
  105.5 0.0 copy-start
  105.5 1.7 copy.36
  107.2 63.8 %all-gather.10.cloned.1.call-done = bf16[2048,1024]{1,0:T(8,128)(2,1)} async-done(((bf16[256,1024]{1,0:T(8,128)(2,1)}), bf16[2048,1024]{1,0:T(8,128)(2,1)}) %all-gather.10.cloned.1.call-update) | async-done | bytes 4194320 | tf_op jit(solution)/shard_map/all_gather | solution.py:83
  171.0 75.1 %all-gather.14.cloned.1.call-done = bf16[1024,2048]{1,0:T(8,128)(2,1)} async-done(((bf16[1024,256]{1,0:T(8,128)(2,1)}), bf16[1024,2048]{1,0:T(8,128)(2,1)}) %all-gather.14.cloned.1.call-update) | async-done | bytes 4194320 | tf_op jit(solution)/shard_map/all_gather | solution.py:88
  246.1 0.0 copy-done
  246.1 9.0 %convolution_convert_fusion = bf16[384,2048]{1,0:T(8,128)(2,1)} fusion(bf16[1024,2048]{1,0:T(8,128)(2,1)} %all-gather.14.cloned.1.call-done, f32[48,8,8,128]{3,2,1,0:T(8,128)} %bitcast.33, bf16[2048,1024]{1,0:T(8,128)(2,1)} %all-gather.10.cloned.1.call-done, bf16[384,2048]{1,0:T(8,128)(2,1)S(1)} %copy-done, f32[2048]{0:T(1024)S(1)} %copy-done.6, ...), kind=kOutput, calls=%fused_computation.13 | convolution fusion | flops 3229089792 | bytes 13116928 | tf_op jit(solution)/shard_map/dot_general | solution.py:58
  255.1 0.0 copy-start.2
  255.1 0.0 copy-start.3
  255.1 0.0 all-reduce.4.cloned.1.call-update
  255.1 0.0 all-gather.16.cloned.1.call-start
  255.2 0.5 all-gather.16.cloned.1.call-update
  255.7 0.0 all-gather.18.cloned.1.call-start
  255.8 0.7 all-gather.18.cloned.1.call-update
  256.5 0.0 all-gather.20.cloned.1.call-start
  256.5 0.7 all-gather.20.cloned.1.call-update
  257.2 0.2 reduce-scatter.2.cloned.1.call-start
  257.4 0.0 copy-done.2
  257.5 0.0 copy-done.3
  257.5 0.1 convert_reduce_fusion.2
  257.6 0.0 copy-start.7
  257.6 16.2 %all-reduce.4.cloned.1.call-done = bf16[384,2048]{1,0:T(8,128)(2,1)} async-done(((bf16[384,2048]{1,0:T(8,128)(2,1)}), bf16[384,2048]{1,0:T(8,128)(2,1)}) %all-reduce.4.cloned.1.call-update) | async-done | bytes 1572880 | tf_op jit(solution)/shard_map/psum | solution.py:89
  273.8 2.1 fusion
  276.0 99.8 %all-gather.16.cloned.1.call-done = bf16[2048,1536]{1,0:T(8,128)(2,1)} async-done(((bf16[256,1536]{1,0:T(8,128)(2,1)}), bf16[2048,1536]{1,0:T(8,128)(2,1)}) %all-gather.16.cloned.1.call-update) | async-done | bytes 6291472 | tf_op jit(solution)/shard_map/all_gather | solution.py:96
  375.8 0.0 copy-done.7
  375.8 6.8 %fusion.64 = f32[384,1536]{1,0:T(8,128)} fusion(bf16[2048,1536]{1,0:T(8,128)(2,1)} %all-gather.16.cloned.1.call-done, bf16[384,2048]{1,0:T(8,128)(2,1)S(1)} %get-tuple-element.12, f32[2048]{0:T(1024)S(1)} %copy-done.7, f32[384]{0:T(512)S(1)} %add_rsqrt_fusion), kind=kOutput, calls=%fused_computation.67 | convolution fusion | flops 2419064832 | bytes 10233344 | tf_op jit(solution)/shard_map/dot_general | solution.py:52
  382.6 92.2 %all-gather.18.cloned.1.call-done = bf16[2048,1536]{1,0:T(8,128)(2,1)} async-done(((bf16[256,1536]{1,0:T(8,128)(2,1)}), bf16[2048,1536]{1,0:T(8,128)(2,1)}) %all-gather.18.cloned.1.call-update) | async-done | bytes 6291472 | tf_op jit(solution)/shard_map/all_gather | solution.py:97
  474.9 6.9 %fusion.62 = f32[384,1536]{1,0:T(8,128)} fusion(bf16[2048,1536]{1,0:T(8,128)(2,1)} %all-gather.18.cloned.1.call-done, bf16[384,2048]{1,0:T(8,128)(2,1)S(1)} %get-tuple-element.12, f32[2048]{0:T(1024)S(1)} %copy-done.7, f32[384]{0:T(512)S(1)} %add_rsqrt_fusion), kind=kOutput, calls=%fused_computation.66 | convolution fusion | flops 2419064832 | bytes 10233344 | tf_op jit(solution)/shard_map/dot_general | solution.py:53
  481.7 92.9 %all-gather.20.cloned.1.call-done = bf16[1536,2048]{1,0:T(8,128)(2,1)} async-done(((bf16[1536,256]{1,0:T(8,128)(2,1)}), bf16[1536,2048]{1,0:T(8,128)(2,1)}) %all-gather.20.cloned.1.call-update) | async-done | bytes 6291472 | tf_op jit(solution)/shard_map/all_gather | solution.py:103
  574.6 12.5 %convolution_convert_fusion.1 = bf16[384,2048]{1,0:T(8,128)(2,1)} fusion(bf16[1536,2048]{1,0:T(8,128)(2,1)} %all-gather.20.cloned.1.call-done, f32[384,1536]{1,0:T(8,128)} %fusion.62, f32[384,1536]{1,0:T(8,128)} %fusion.64, f32[1536]{0:T(1024)S(1)} %get-tuple-element.9, f32[1536]{0:T(1024)S(1)} %get-tuple-element.10, f32[1536]{0:T(1024)S(1)} %get-tuple-element.8, ...), kind=kOutput, calls=%fused_computation.14 | convolution fusion | flops 2428502016 | bytes 12619776 | tf_op jit(solution)/shard_map/dot_general | solution.py:58
  587.1 0.0 reduce-scatter.2.cloned.1.call-update
  587.1 7.3 %reduce-scatter.2.cloned.1.call-done = bf16[384,1024]{1,0:T(8,128)(2,1)} async-done(((bf16[384,2048]{1,0:T(8,128)(2,1)}), bf16[384,1024]{1,0:T(8,128)(2,1)}) %reduce-scatter.2.cloned.1.call-update) | async-done | bytes 786448 | tf_op jit(solution)/shard_map/reduce_scatter | solution.py:104
  594.4 2.3 add_convert_fusion
  (7 shorter events, 0.1 us)
Async XLA Ops:
  6.5 91.0 %copy-start.6 = (f32[2048]{0:T(1024)S(1)}, f32[2048]{0:T(1024)}, u32[]{:S(2)}) copy-start(f32[2048]{0:T(1024)} %param.15) | copy-start | bytes 24580
  6.5 14.9 %all-gather.8.cloned.1.call-start = ((), (), s32[]{:S(2)}) async-start(), calls=%async_computation.1 | async-start | bytes 2359296 | tf_op jit(solution)/shard_map/all_gather | solution.py:78
  7.3 90.3 %all-gather.12.cloned.1.call-start = ((), (), s32[]{:S(2)}) async-start(), calls=%async_computation.3 | async-start | bytes 4718592 | tf_op jit(solution)/shard_map/all_gather | solution.py:84
  8.0 163.0 %all-gather.10.cloned.1.call-start = ((), (), s32[]{:S(2)}) async-start(), calls=%async_computation.2 | async-start | bytes 4718592 | tf_op jit(solution)/shard_map/all_gather | solution.py:83
  8.7 237.4 %all-gather.14.cloned.1.call-start = ((), (), s32[]{:S(2)}) async-start(), calls=%async_computation.4 | async-start | bytes 4718592 | tf_op jit(solution)/shard_map/all_gather | solution.py:88
  9.3 264.5 %all-reduce.4.cloned.1.call-start = ((), (), s32[]{:S(2)}) async-start(), calls=%async_computation.5 | async-start | bytes 3145728 | tf_op jit(solution)/shard_map/psum | solution.py:89
  103.4 1.6 copy-start.1
  103.4 1.6 copy-start.4
  103.4 1.6 copy-start.5
  105.5 140.6 %copy-start = (bf16[384,2048]{1,0:T(8,128)(2,1)S(1)}, bf16[384,2048]{1,0:T(8,128)(2,1)}, u32[]{:S(2)}) copy-start(bf16[384,2048]{1,0:T(8,128)(2,1)} %all-gather.8.cloned.1.call-done) | copy-start | bytes 4718596
  255.1 2.3 copy-start.2
  255.1 2.3 copy-start.3
  255.1 120.6 %all-gather.16.cloned.1.call-start = ((), (), s32[]{:S(2)}) async-start(), calls=%async_computation.6 | async-start | bytes 7077888 | tf_op jit(solution)/shard_map/all_gather | solution.py:96
  255.7 219.1 %all-gather.18.cloned.1.call-start = ((), (), s32[]{:S(2)}) async-start(), calls=%async_computation.7 | async-start | bytes 7077888 | tf_op jit(solution)/shard_map/all_gather | solution.py:97
  256.5 318.1 %all-gather.20.cloned.1.call-start = ((), (), s32[]{:S(2)}) async-start(), calls=%async_computation.8 | async-start | bytes 7077888 | tf_op jit(solution)/shard_map/all_gather | solution.py:103
  257.2 337.2 %reduce-scatter.2.cloned.1.call-start = ((), (), s32[]{:S(2)}) async-start(), calls=%async_computation.9 | async-start | bytes 2359296 | tf_op jit(solution)/shard_map/reduce_scatter | solution.py:104
  257.6 118.2 %copy-start.7 = (f32[2048]{0:T(1024)S(1)}, f32[2048]{0:T(1024)}, u32[]{:S(2)}) copy-start(f32[2048]{0:T(1024)} %param.22) | copy-start | bytes 24580
Sparse Core Ops, SparseCore 0:
  8.9 12.5 all-gather.7
  23.6 73.9 all-gather.11
  99.7 71.3 all-gather.9
  172.9 73.1 all-gather.13
  255.3 18.5 all-reduce.3
  275.9 99.8 all-gather.15
  377.9 96.8 all-gather.17
  476.9 97.6 all-gather.19
  587.2 7.1 reduce-scatter.1
where the time goes:
time: 604 us; the launch traced here: 603 us
  waiting for transfers between devices  538 us (89%)
  matrix products  40.4 us (7%)
  between operations  13.4 us (2%)
  other arithmetic  7.79 us (1%)
    all_gather x1, waiting for transfers between devices, on_device(): lax.all_gather(w_gate, 'fs', axis=0, tiled=True)  99.8 us
    all_gather x1, waiting for transfers between devices, on_device(): lax.all_gather(w_down, 'fs', axis=1, tiled=True)  92.9 us
    all_gather x1, waiting for transfers between devices, on_device(): lax.all_gather(w_value, 'fs', axis=0, tiled=True)  92.2 us
    all_gather x1, waiting for transfers between devices, on_device(): lax.all_gather(w_mix_out, 'fs', axis=1, tiled=True)  75.1 us
    all_gather x1, waiting for transfers between devices, on_device(): lax.all_gather(w_v, 'fs', axis=0, tiled=True)  74.3 us
    all_gather x1, waiting for transfers between devices, on_device(): lax.all_gather(w_u, 'fs', axis=0, tiled=True)  63.8 us
    dot_general x2, matrix products, project_with(): return jnp.dot(operand, weight_piece, preferred_element_type=jnp.float32)  21.5 us
    psum x1, waiting for transfers between devices, on_device(): lax.psum(mixer_terms.astype(jnp.bfloat16), 'tp').astype(jnp.float32)  16.2 us
  transfers between devices with their start and end apart: 9, of which 9 were waited for; matrix products, arithmetic and copies ran while one was open for 5% of the time, Pallas kernels for 0%

commit v1 on v0

--- a/solution.py
+++ b/solution.py
@@ -58,6 +58,20 @@
     return jnp.dot(operand, weight_piece, preferred_element_type=jnp.float32)
 
 
+def own_half(array, axis):
+    share = array.shape[axis] // lax.axis_size("rep")
+    return lax.dynamic_slice_in_dim(array, lax.axis_index("rep") * share, share, axis)
+
+
+def share_tokens(own):
+    return lax.all_gather(lax.all_gather(own, "rep", axis=0, tiled=True), "tp", axis=1, tiled=True)
+
+
+def scatter_sums(terms):
+    part = lax.psum_scatter(terms.astype(jnp.bfloat16), "tp", scatter_dimension=1, tiled=True)
+    return lax.psum_scatter(part, "rep", scatter_dimension=0, tiled=True).astype(jnp.float32)
+
+
 def on_device(
     tokens,
     mix_gain,
@@ -74,37 +88,34 @@
     taps_value,
     w_down,
 ):
-    own_width = tokens.shape[1]
-    features = lax.all_gather(tokens, "tp", axis=1, tiled=True)
+    seq_len = tokens.shape[0]
+    features = share_tokens(tokens)
+    w_in = lax.all_gather(
+        jnp.concatenate((own_half(w_u, 1), own_half(w_v, 1)), 1), "fs", axis=0, tiled=True
+    )
+    w_out = lax.all_gather(own_half(w_mix_out, 0), "fs", axis=1, tiled=True)
+    w_up = lax.all_gather(
+        jnp.concatenate((own_half(w_gate, 1), own_half(w_value, 1)), 1), "fs", axis=0, tiled=True
+    )
+    w_dn = lax.all_gather(own_half(w_down, 0), "fs", axis=1, tiled=True)
     normed = rms_scale(features, mix_gain)
-    u_pre, v_pre = add_pair(
-        normed,
-        (
-            lax.all_gather(w_u, "fs", axis=0, tiled=True),
-            lax.all_gather(w_v, "fs", axis=0, tiled=True),
-        ),
+    u_pre, v_pre = jnp.split(project_with(normed, w_in), 2, 1)
+    hidden = spatial_mix(
+        u_pre, v_pre, own_half(norm_gain, 0), own_half(mix_weight, 0), own_half(mix_bias, 0)
     )
-    hidden = spatial_mix(u_pre, v_pre, norm_gain, mix_weight, mix_bias)
-    mixer_terms = project_with(hidden, lax.all_gather(w_mix_out, "fs", axis=1, tiled=True))
-    mixer_full = lax.psum(mixer_terms.astype(jnp.bfloat16), "tp").astype(jnp.float32)
-    middle = (features.astype(jnp.float32) + mixer_full).astype(jnp.bfloat16)
-    middle_own = lax.dynamic_slice_in_dim(middle, lax.axis_index("tp") * own_width, own_width, 1)
-    normed_mid = rms_scale(middle, ffn_gain)
-    gate_pre, value_pre = add_pair(
-        normed_mid,
-        (
-            lax.all_gather(w_gate, "fs", axis=0, tiled=True),
-            lax.all_gather(w_value, "fs", axis=0, tiled=True),
-        ),
-    )
+    mixer_own = scatter_sums(project_with(hidden, w_out))
+    middle_own = (tokens.astype(jnp.float32) + mixer_own).astype(jnp.bfloat16)
+    normed_mid = rms_scale(share_tokens(middle_own), ffn_gain)
+    gate_pre, value_pre = jnp.split(project_with(normed_mid, w_up), 2, 1)
+    sequences = (-1, seq_len, gate_pre.shape[1])
+    conv = jax.vmap(causal_taps, (0, None))
     activation = (
-        jax.nn.gelu(causal_taps(gate_pre, taps_gate)) * causal_taps(value_pre, taps_value)
+        jax.nn.gelu(conv(gate_pre.reshape(sequences), own_half(taps_gate, 1)))
+        * conv(value_pre.reshape(sequences), own_half(taps_value, 1))
     ).astype(jnp.bfloat16)
-    down_terms = project_with(activation, lax.all_gather(w_down, "fs", axis=1, tiled=True))
-    channel_part = lax.psum_scatter(
-        down_terms.astype(jnp.bfloat16), "tp", scatter_dimension=1, tiled=True
-    ).astype(jnp.float32)
-    return (middle_own.astype(jnp.float32) + channel_part).astype(jnp.bfloat16)
+    activation = activation.reshape(gate_pre.shape)
+    channel_own = scatter_sums(project_with(activation, w_dn))
+    return (middle_own.astype(jnp.float32) + channel_own).astype(jnp.bfloat16)
 
 
 def solution(mesh):

time: 604 us -> 487 us (0.81)
  waiting for transfers between devices: 538 us -> 412 us
  matrix products: 40.4 us -> 28.3 us
  other arithmetic: 7.79 us -> 18.9 us
  local copies, waits for them, and re-layouts: 2.98 us -> 12.8 us
    all_gather x7 -> x8, waiting for transfers between devices: 510 us -> 334 us  [the longest x1 99.5 us: on_device(): lax.all_gather(jnp.concatenate((own_half(w_gate, 1), own_half(w_value, 1)...]
    reduce_scatter x1 -> x4, waiting for transfers between devices: 7.28 us -> 77.5 us  [the longest x2 59 us: scatter_sums(): lax.psum_scatter(part, 'rep', scatter_dimension=0, tiled=True)]
    dot_general x3 -> x0, matrix products: 18.5 us -> none  [the longest x2 11.6 us: add_pair(): second = jnp.dot(operand, pieces[1], preferred_element_type=jnp.float32)]
    psum x1 -> x0, waiting for transfers between devices: 16.2 us -> none  [on_device(): lax.psum(mixer_terms.astype(jnp.bfloat16), 'tp').astype(jnp.float32)]
    dot_general x2 -> x4, matrix products: 21.5 us -> 26.5 us  [project_with(): return jnp.dot(operand, weight_piece, preferred_element_type=jnp.float32)]
  transfers between devices with their start and end apart: 9 -> 12, of which waited for: 9 -> 12; matrix products, arithmetic and copies ran while one was open for 5% -> 8% of each run, Pallas kernels for 0% -> 0%
where the time goes in v1:
time: 487 us
  waiting for transfers between devices  412 us (85%)
  matrix products  28.3 us (6%)
  other arithmetic  18.9 us (4%)
  between operations  13.9 us (3%)
  local copies, waits for them, and re-layouts  12.8 us (3%)
    all_gather x1, waiting for transfers between devices, on_device(): lax.all_gather(jnp.concatenate((own_half(w_gate, 1), own_half(w_value, 1)...  99.5 us
    all_gather x1, waiting for transfers between devices, on_device(): lax.all_gather(jnp.concatenate((own_half(w_u, 1), own_half(w_v, 1)), 1),...  73.5 us
    reduce_scatter x2, waiting for transfers between devices, scatter_sums(): lax.psum_scatter(part, 'rep', scatter_dimension=0, tiled=True)  59 us
    all_gather x2, waiting for transfers between devices, share_tokens(): lax.all_gather(own, 'rep', axis=0, tiled=True)  58.8 us
    all_gather x1, waiting for transfers between devices, on_device(): w_dn = lax.all_gather(own_half(w_down, 0), 'fs', axis=1, tiled=True)  51.9 us
    all_gather x1, waiting for transfers between devices, on_device(): w_out = lax.all_gather(own_half(w_mix_out, 0), 'fs', axis=1, tiled=True)  27.1 us
    dot_general x4, matrix products, project_with(): return jnp.dot(operand, weight_piece, preferred_element_type=jnp.float32)  26.5 us
    all_gather x2, waiting for transfers between devices, share_tokens(): lax.all_gather(lax.all_gather(own, 'rep', axis=0, tiled=True), 'tp', axis...  23 us
  transfers between devices with their start and end apart: 12, of which 12 were waited for; matrix products, arithmetic and copies ran while one was open for 8% of the time, Pallas kernels for 0%

profile of v1, /device:TPU:0, one launch (start us, length us, event | category | flops | bytes accessed | tf_op | source)
XLA Modules:
  0.0 486.7 jit_solution(4065928270848672887)
XLA Ops:
  6.5 0.0 all-gather.9.cloned.1.call-start
  6.6 0.7 all-gather.9.cloned.1.call-update
  7.3 0.0 all-gather.11.cloned.1.call-start
  7.3 31.5 %all-gather.9.cloned.1.call-done = bf16[768,1024]{1,0:T(8,128)(2,1)} async-done(((bf16[384,1024]{1,0:T(8,128)(2,1)}), bf16[768,1024]{1,0:T(8,128)(2,1)}) %all-gather.9.cloned.1.call-update) | async-done | bytes 1572880 | tf_op jit(solution)/shard_map/all_gather | solution.py:67
  38.8 0.0 all-gather.11.cloned.1.call-update
  38.9 0.0 all-gather.13.cloned.1.call-start
  39.0 0.9 pad_maximum_fusion.1
  39.9 0.0 all-gather.15.cloned.1.call-start
  39.9 0.7 constant_dynamic-slice_fusion.3
  40.7 0.0 all-gather.15.cloned.1.call-update
  40.7 0.0 reduce-scatter.5.cloned.1.call-start
  40.7 0.1 dynamic-slice_bitcast_fusion
  40.8 11.7 %all-gather.11.cloned.1.call-done = bf16[768,2048]{1,0:T(8,128)(2,1)} async-done(((bf16[768,1024]{1,0:T(8,128)(2,1)}), bf16[768,2048]{1,0:T(8,128)(2,1)}) %all-gather.11.cloned.1.call-update) | async-done | bytes 3145744 | tf_op jit(solution)/shard_map/all_gather | solution.py:67
  52.5 2.6 fusion
  55.1 73.5 %all-gather.13.cloned.1.call-done = bf16[2048,1024]{1,0:T(8,128)(2,1)} async-done(((bf16[256,1024]{1,0:T(8,128)(2,1)}), bf16[2048,1024]{1,0:T(8,128)(2,1)}) %all-gather.13.cloned.1.call-update) | async-done | bytes 4194320 | tf_op jit(solution)/shard_map/all_gather | solution.py:93
  128.7 6.2 %fusion.8 = f32[768,1024]{1,0:T(8,128)S(1)} fusion(bf16[2048,1024]{1,0:T(8,128)(2,1)} %all-gather.13.cloned.1.call-done, bf16[768,2048]{1,0:T(8,128)(2,1)} %all-gather.11.cloned.1.call-done, f32[2048]{0:T(1024)S(1)} %copy-done.16, f32[768]{0:T(1024)S(1)} %add_rsqrt_fusion.2), kind=kOutput, calls=%fused_computation.14 | convolution fusion | flops 3227516928 | bytes 10497024 | tf_op jit(solution)/shard_map/dot_general | solution.py:58
  134.9 1.6 copy-done.5
  136.6 1.6 fusion.38
  138.2 1.8 reshape.119
  140.0 2.8 reshape.118
  142.8 0.9 reduce_sum.37
  143.7 2.3 multiply_reduce_fusion
  146.0 0.1 add_rsqrt_fusion
  146.0 0.2 copy.37
  146.2 0.2 copy.38
  146.4 0.9 copy-done.3
  147.4 1.6 copy.27
  149.0 1.8 bitcast_add_fusion
  150.8 1.6 copy.30
  152.4 27.1 %all-gather.15.cloned.1.call-done = bf16[512,2048]{1,0:T(8,128)(2,1)} async-done(((bf16[512,256]{1,0:T(8,128)(2,1)}), bf16[512,2048]{1,0:T(8,128)(2,1)}) %all-gather.15.cloned.1.call-update) | async-done | bytes 2097168 | tf_op jit(solution)/shard_map/all_gather | solution.py:96
  179.5 6.2 %convolution_convert_fusion = bf16[768,2048]{1,0:T(8,128)(2,1)} fusion(bf16[512,2048]{1,0:T(8,128)(2,1)} %all-gather.15.cloned.1.call-done, f32[96,8,4,128]{3,2,1,0:T(4,128)} %bitcast.31, f32[768,1024]{1,0:T(8,128)} %copy-done.5), kind=kOutput, calls=%fused_computation.11 | convolution fusion | flops 1616117760 | bytes 8388608 | tf_op jit(solution)/shard_map/dot_general | solution.py:58
  185.7 0.0 reduce-scatter.5.cloned.1.call-update
  185.7 0.0 reduce-scatter.7.cloned.1.call-start
  185.8 9.2 %reduce-scatter.5.cloned.1.call-done = bf16[768,1024]{1,0:T(8,128)(2,1)} async-done(((bf16[768,2048]{1,0:T(8,128)(2,1)}), bf16[768,1024]{1,0:T(8,128)(2,1)}) %reduce-scatter.5.cloned.1.call-update) | async-done | bytes 1572880 | tf_op jit(solution)/shard_map/reduce_scatter | solution.py:71
  195.0 0.0 reduce-scatter.7.cloned.1.call-update
  195.1 0.0 all-gather.17.cloned.1.call-start
  195.1 29.5 %reduce-scatter.7.cloned.1.call-done = bf16[384,1024]{1,0:T(8,128)(2,1)} async-done(((bf16[768,1024]{1,0:T(8,128)(2,1)}), bf16[384,1024]{1,0:T(8,128)(2,1)}) %reduce-scatter.7.cloned.1.call-update) | async-done | bytes 786448 | tf_op jit(solution)/shard_map/reduce_scatter | solution.py:72
  224.6 2.4 add_convert_fusion.1
  226.9 0.0 all-gather.17.cloned.1.call-update
  226.9 0.0 all-gather.19.cloned.1.call-start
  227.0 27.3 %all-gather.17.cloned.1.call-done = bf16[768,1024]{1,0:T(8,128)(2,1)} async-done(((bf16[384,1024]{1,0:T(8,128)(2,1)}), bf16[768,1024]{1,0:T(8,128)(2,1)}) %all-gather.17.cloned.1.call-update) | async-done | bytes 1572880 | tf_op jit(solution)/shard_map/all_gather | solution.py:67
  254.3 0.0 all-gather.19.cloned.1.call-update
  254.3 0.0 all-gather.21.cloned.1.call-start
  254.4 0.1 constant_dynamic-slice_fusion.1
  254.5 0.9 pad_maximum_fusion
  255.4 0.0 all-gather.21.cloned.1.call-update
  255.5 0.0 all-gather.23.cloned.1.call-start
  255.5 0.8 constant_dynamic-slice_fusion
  256.3 0.0 all-gather.23.cloned.1.call-update
  256.3 0.2 reduce-scatter.9.cloned.1.call-start
  256.6 0.1 fusion.54
  256.7 11.3 %all-gather.19.cloned.1.call-done = bf16[768,2048]{1,0:T(8,128)(2,1)} async-done(((bf16[768,1024]{1,0:T(8,128)(2,1)}), bf16[768,2048]{1,0:T(8,128)(2,1)}) %all-gather.19.cloned.1.call-update) | async-done | bytes 3145744 | tf_op jit(solution)/shard_map/all_gather | solution.py:67
  268.0 2.6 fusion.3
  270.6 99.5 %all-gather.21.cloned.1.call-done = bf16[2048,1536]{1,0:T(8,128)(2,1)} async-done(((bf16[256,1536]{1,0:T(8,128)(2,1)}), bf16[2048,1536]{1,0:T(8,128)(2,1)}) %all-gather.21.cloned.1.call-update) | async-done | bytes 6291472 | tf_op jit(solution)/shard_map/all_gather | solution.py:97
  370.1 8.2 %fusion.6 = f32[768,1536]{1,0:T(8,128)S(1)} fusion(bf16[2048,1536]{1,0:T(8,128)(2,1)} %all-gather.21.cloned.1.call-done, bf16[768,2048]{1,0:T(8,128)(2,1)} %all-gather.19.cloned.1.call-done, f32[2048]{0:T(1024)S(1)} %copy-done.17, f32[768]{0:T(1024)S(1)} %add_rsqrt_fusion.1), kind=kOutput, calls=%fused_computation.13 | convolution fusion | flops 4838129664 | bytes 14167040 | tf_op jit(solution)/shard_map/dot_general | solution.py:58
  378.3 0.4 fusion.65
  378.7 2.3 fusion.22
  381.0 51.9 %all-gather.23.cloned.1.call-done = bf16[768,2048]{1,0:T(8,128)(2,1)} async-done(((bf16[768,256]{1,0:T(8,128)(2,1)}), bf16[768,2048]{1,0:T(8,128)(2,1)}) %all-gather.23.cloned.1.call-update) | async-done | bytes 3145744 | tf_op jit(solution)/shard_map/all_gather | solution.py:100
  432.9 5.8 %convolution_convert_fusion.1 = bf16[768,2048]{1,0:T(8,128)(2,1)} fusion(bf16[768,768]{1,0:T(8,128)(2,1)S(1)} %bitcast.33, bf16[768,2048]{1,0:T(8,128)(2,1)} %all-gather.23.cloned.1.call-done), kind=kOutput, calls=%fused_computation.12 | convolution fusion | flops 2417491968 | bytes 7471104 | tf_op jit(solution)/shard_map/dot_general | solution.py:58
  438.7 0.0 reduce-scatter.9.cloned.1.call-update
  438.7 0.0 reduce-scatter.11.cloned.1.call-start
  438.8 9.2 %reduce-scatter.9.cloned.1.call-done = bf16[768,1024]{1,0:T(8,128)(2,1)} async-done(((bf16[768,2048]{1,0:T(8,128)(2,1)}), bf16[768,1024]{1,0:T(8,128)(2,1)}) %reduce-scatter.9.cloned.1.call-update) | async-done | bytes 1572880 | tf_op jit(solution)/shard_map/reduce_scatter | solution.py:71
  448.0 29.5 %reduce-scatter.11.cloned.1.call-done = bf16[384,1024]{1,0:T(8,128)(2,1)} async-done(((bf16[768,1024]{1,0:T(8,128)(2,1)}), bf16[384,1024]{1,0:T(8,128)(2,1)}) %reduce-scatter.11.cloned.1.call-update) | async-done | bytes 786448 | tf_op jit(solution)/shard_map/reduce_scatter | solution.py:72
  477.6 2.3 add_convert_fusion
  (42 shorter events, 0.2 us)
Async XLA Ops:
  6.5 249.0 %copy-start = (bf16[1536,256]{1,0:T(8,128)(2,1)S(1)}, bf16[1536,256]{1,0:T(8,128)(2,1)}, u32[]{:S(2)}) copy-start(bf16[1536,256]{1,0:T(8,128)(2,1)} %param.27) | copy-start | bytes 2359300
  6.5 32.4 %copy-start.10 = (bf16[256,1024]{1,0:T(8,128)(2,1)S(1)}, bf16[256,1024]{1,0:T(8,128)(2,1)}, u32[]{:S(2)}) copy-start(bf16[256,1024]{1,0:T(8,128)(2,1)} %param.16) | copy-start | bytes 1572868
  6.5 32.4 %copy-start.9 = (bf16[256,1024]{1,0:T(8,128)(2,1)S(1)}, bf16[256,1024]{1,0:T(8,128)(2,1)}, u32[]{:S(2)}) copy-start(bf16[256,1024]{1,0:T(8,128)(2,1)} %param.17) | copy-start | bytes 1572868
  6.5 33.4 %copy-start.8 = (bf16[1024,256]{1,0:T(8,128)(2,1)S(1)}, bf16[1024,256]{1,0:T(8,128)(2,1)}, u32[]{:S(2)}) copy-start(bf16[1024,256]{1,0:T(8,128)(2,1)} %param.21) | copy-start | bytes 1572868
  6.5 32.3 %all-gather.9.cloned.1.call-start = ((), (), s32[]{:S(2)}) async-start(), calls=%async_computation.4 | async-start | bytes 2359296 | tf_op jit(solution)/shard_map/all_gather | solution.py:67
  7.3 45.3 %all-gather.11.cloned.1.call-start = ((), (), s32[]{:S(2)}) async-start(), calls=%async_computation.5 | async-start | bytes 4718592 | tf_op jit(solution)/shard_map/all_gather | solution.py:67
  38.8 1.9 copy-start.14
  38.8 2.0 copy-start.15
  38.9 89.8 %all-gather.13.cloned.1.call-start = ((), (), s32[]{:S(2)}) async-start(), calls=%async_computation.6 | async-start | bytes 4718592 | tf_op jit(solution)/shard_map/all_gather | solution.py:93
  39.8 88.8 %copy-start.16 = (f32[2048]{0:T(1024)S(1)}, f32[2048]{0:T(1024)}, u32[]{:S(2)}) copy-start(f32[2048]{0:T(1024)} %param.15) | copy-start | bytes 24580
  39.9 139.6 %all-gather.15.cloned.1.call-start = ((), (), s32[]{:S(2)}) async-start(), calls=%async_computation.7 | async-start | bytes 2359296 | tf_op jit(solution)/shard_map/all_gather | solution.py:96
  40.7 154.3 %reduce-scatter.5.cloned.1.call-start = ((), (), s32[]{:S(2)}) async-start(), calls=%async_computation.8 | async-start | bytes 4718592 | tf_op jit(solution)/shard_map/reduce_scatter | solution.py:71
  134.9 1.7 copy-start.5
  146.0 1.4 copy-start.3
  146.0 3.0 copy-start.11
  185.7 38.9 %copy-start.4 = (bf16[384,1024]{1,0:T(8,128)(2,1)S(1)}, bf16[384,1024]{1,0:T(8,128)(2,1)}, u32[]{:S(2)}) copy-start(bf16[384,1024]{1,0:T(8,128)(2,1)} %param.14) | copy-start | bytes 2359300
  185.7 38.9 %reduce-scatter.7.cloned.1.call-start = ((), (), s32[]{:S(2)}) async-start(), calls=%async_computation.9 | async-start | bytes 2359296 | tf_op jit(solution)/shard_map/reduce_scatter | solution.py:72
  195.0 59.4 %copy-start.6 = (bf16[256,1536]{1,0:T(8,128)(2,1)S(1)}, bf16[256,1536]{1,0:T(8,128)(2,1)}, u32[]{:S(2)}) copy-start(bf16[256,1536]{1,0:T(8,128)(2,1)} %param.24) | copy-start | bytes 2359300
  195.0 59.4 %copy-start.7 = (bf16[256,1536]{1,0:T(8,128)(2,1)S(1)}, bf16[256,1536]{1,0:T(8,128)(2,1)}, u32[]{:S(2)}) copy-start(bf16[256,1536]{1,0:T(8,128)(2,1)} %param.23) | copy-start | bytes 2359300
  195.1 59.3 %all-gather.17.cloned.1.call-start = ((), (), s32[]{:S(2)}) async-start(), calls=%async_computation.10 | async-start | bytes 2359296 | tf_op jit(solution)/shard_map/all_gather | solution.py:67
  226.9 41.1 %all-gather.19.cloned.1.call-start = ((), (), s32[]{:S(2)}) async-start(), calls=%async_computation.11 | async-start | bytes 4718592 | tf_op jit(solution)/shard_map/all_gather | solution.py:67
  254.3 115.8 %all-gather.21.cloned.1.call-start = ((), (), s32[]{:S(2)}) async-start(), calls=%async_computation.12 | async-start | bytes 7077888 | tf_op jit(solution)/shard_map/all_gather | solution.py:97
  254.4 2.2 copy-start.12
  254.4 2.2 copy-start.13
  255.5 114.6 %copy-start.17 = (f32[2048]{0:T(1024)S(1)}, f32[2048]{0:T(1024)}, u32[]{:S(2)}) copy-start(f32[2048]{0:T(1024)} %param.22) | copy-start | bytes 24580
  255.5 177.4 %all-gather.23.cloned.1.call-start = ((), (), s32[]{:S(2)}) async-start(), calls=%async_computation.13 | async-start | bytes 3538944 | tf_op jit(solution)/shard_map/all_gather | solution.py:100
  256.3 191.7 %reduce-scatter.9.cloned.1.call-start = ((), (), s32[]{:S(2)}) async-start(), calls=%async_computation.14 | async-start | bytes 4718592 | tf_op jit(solution)/shard_map/reduce_scatter | solution.py:71
  438.7 38.9 %copy-start.2 = (bf16[384,1024]{1,0:T(8,128)(2,1)S(1)}, bf16[384,1024]{1,0:T(8,128)(2,1)}, u32[]{:S(2)}) copy-start(bf16[384,1024]{1,0:T(8,128)(2,1)} %add_convert_fusion.1) | copy-start | bytes 2359300
  438.7 41.2 %copy-start.1 = (bf16[1536,256]{1,0:T(8,128)(2,1)S(1)}, bf16[1536,256]{1,0:T(8,128)(2,1)}, u32[]{:S(2)}) copy-start(bf16[1536,256]{1,0:T(8,128)(2,1)} %param.27) | copy-start | bytes 2359300
  438.7 38.8 %reduce-scatter.11.cloned.1.call-start = ((), (), s32[]{:S(2)}) async-start(), calls=%async_computation.15 | async-start | bytes 2359296 | tf_op jit(solution)/shard_map/reduce_scatter | solution.py:72
Sparse Core Ops, SparseCore 0:
  8.9 29.8 all-gather.8
  40.4 12.1 all-gather.10
  54.7 73.9 all-gather.12
  130.6 48.8 all-gather.14
  185.8 9.1 reduce-scatter.4
  197.1 27.4 reduce-scatter.6
  227.1 27.1 all-gather.16
  255.9 12.1 all-gather.18
  270.2 99.8 all-gather.20
  372.0 60.8 all-gather.22
  438.8 9.1 reduce-scatter.8
  450.1 27.4 reduce-scatter.10

commit v2 on v0

v2 whole, which is shorter than its diff:
```python
import functools

import jax
import jax.numpy as jnp
from jax import lax
from jax.experimental import pallas as pl
from jax.experimental.pallas import tpu as pltpu
from jax.sharding import PartitionSpec as P

EPS_RMS = 1e-06
EPS_LN = 1e-05
F32 = jnp.float32
BF16 = jnp.bfloat16
MESH = pl.DeviceIdType.MESH


def own_half(array, axis):
    share = array.shape[axis] // lax.axis_size("rep")
    return lax.dynamic_slice_in_dim(array, lax.axis_index("rep") * share, share, axis)


def layer_kernel(
    n, nr, nt,
    tok, mix_gain, w_in, norm_gain, mixw, bias, w_out, ffn_gain, w_up, taps_g, taps_v, w_dn,
    out,
    g_in, g_out, g_up, g_dn, feat, feat2, normed, uv, hidden, gv, act, part1, part2, got1, got2,
    w_send, w_recv, w_local, f_send, f_recv, p_send, p_recv,
):
    rep, fs, tp = lax.axis_index("rep"), lax.axis_index("fs"), lax.axis_index("tp")
    seq, own_width = tok.shape
    nz = n // 2
    z, y = fs // 2, fs % 2
    per = n // nt
    depth = normed.shape[2]
    mine = (w_in, w_out, w_up, w_dn)
    gathered = (g_in, g_out, g_up, g_dn)
    offsets = [(a, b) for a in range(nr) for b in range(nt) if (a, b) != (0, 0)]

    def peer(a, b):
        return {"rep": lax.rem(rep + a, nr), "tp": lax.rem(tp + b, nt)}

    barrier = pltpu.get_barrier_semaphore()
    line = (lax.rem(z + 1, nz), lax.rem(z + nz - 1, nz))
    greeted = [{"fs": z * 2 + 1 - y}] + [{"fs": at * 2 + y} for at in line]
    greeted += [peer(a, b) for a, b in offsets]
    for target in greeted:
        pl.semaphore_signal(barrier, inc=1, device_id=target, device_id_type=MESH)
    pl.semaphore_wait(barrier, len(greeted))

    def hop(stage, block, way):
        target = (fs + 2, fs - 2, z * 2 + 1 - y)[way]
        return pltpu.make_async_remote_copy(
            src_ref=gathered[stage].at[block],
            dst_ref=gathered[stage].at[block],
            send_sem=w_send.at[stage, way, block],
            recv_sem=w_recv.at[stage, block],
            device_id={"fs": target},
            device_id_type=MESH,
        )

    def ways(src):
        return (
            jnp.logical_and(src <= z, z < nz - 1),
            jnp.logical_and(src >= z, z > 0),
        )

    def forward(stage, src):
        block = src * 2 + y
        hop(stage, block, 2).start()
        for way, used in enumerate(ways(src)):
            @pl.when(used)
            def _():
                hop(stage, block, way).start()

    def arrived(stage, block):
        hop(stage, block, 2).wait_recv()

    def order(i):
        near = jnp.minimum(z, nz - 1 - z)
        swing = z + ((i + 1) // 2) * (1 - 2 * (i % 2))
        rest = jnp.where(z < nz - 1 - z, i, nz - 1 - i)
        return jnp.where(i <= 2 * near, swing, rest)

    def stage_loop(stage, compute, begin, middle):
        def step(i, _):
            src = order(i)

            @pl.when(i > 0)
            def _():
                arrived(stage, src * 2 + y)
                forward(stage, src)

            compute(src * 2 + y)

            @pl.when(i > 0)
            def _():
                other = order(i - 1) * 2 + 1 - y
                arrived(stage, other)
                compute(other)

            return 0

        lax.fori_loop(begin, nz, step, 0)
        middle()
        last = order(nz - 1) * 2 + 1 - y
        arrived(stage, last)
        compute(last)

    locals_ = [
        pltpu.make_async_copy(mine[k], gathered[k].at[fs], w_local.at[k]) for k in range(4)
    ]
    own_tok = pltpu.make_async_copy(tok, feat.at[rep, tp], w_local.at[4])
    for copy in locals_ + [own_tok]:
        copy.start()

    def share(turn, slabs):
        copies = []
        for k, (a, b) in enumerate(offsets):
            copies.append(
                pltpu.make_async_remote_copy(
                    src_ref=slabs.at[rep, tp],
                    dst_ref=slabs.at[rep, tp],
                    send_sem=f_send.at[turn, k],
                    recv_sem=f_recv.at[turn, k],
                    device_id=peer(a, b),
                    device_id_type=MESH,
                )
            )
        return copies

    def share_wait(turn, slabs):
        for k, (a, b) in enumerate(offsets):
            slab = slabs.at[lax.rem(rep + nr - a, nr), lax.rem(tp + nt - b, nt)]
            pltpu.make_async_remote_copy(
                src_ref=slab, dst_ref=slab, send_sem=f_send.at[turn, k],
                recv_sem=f_recv.at[turn, k], device_id=peer(a, b), device_id_type=MESH,
            ).wait_recv()

    def norm(slabs, gain):
        for r in range(nr):
            total = jnp.zeros((seq, 1), F32)
            for t in range(nt):
                values = slabs[r, t].astype(F32)
                total += jnp.sum(values * values, axis=1, keepdims=True)
            scale = lax.rsqrt(total / (nt * own_width) + EPS_RMS)
            for t in range(nt):
                for j in range(per):
                    values = slabs[r, t, :, j * depth : (j + 1) * depth].astype(F32)
                    normed[t * per + j, r * seq : (r + 1) * seq, :] = (
                        values * scale * gain[t * per + j]
                    ).astype(BF16)

    def piece(turn, part, got, block, r):
        return pltpu.make_async_remote_copy(
            src_ref=part.at[block, r],
            dst_ref=got.at[rep * nt + tp, block % per],
            send_sem=p_send.at[turn, block, r],
            recv_sem=p_recv.at[turn, rep * nt + tp, block % per],
            device_id={"rep": r, "tp": block // per},
            device_id_type=MESH,
        )

    def abroad(block, r):
        return jnp.logical_or(block // per != tp, r != rep)

    def project(turn, left, gathered_w, part, got, block):
        for r in range(nr):
            part[block, r] = jnp.dot(
                left[r], gathered_w[block], preferred_element_type=F32
            ).astype(BF16)

            @pl.when(abroad(block, r))
            def _():
                piece(turn, part, got, block, r).start()

    def collect(turn, part, got, base, emit):
        for j in range(per):
            total = part[tp * per + j, rep].astype(F32)
            for a, b in offsets:
                slot = lax.rem(rep + a, nr) * nt + lax.rem(tp + b, nt)
                landing = got.at[slot, j]
                pltpu.make_async_remote_copy(
                    src_ref=landing, dst_ref=landing, send_sem=p_send.at[turn, 0, 0],
                    recv_sem=p_recv.at[turn, slot, j], device_id=peer(a, b),
                    device_id_type=MESH,
                ).wait_recv()
                total += got[slot, j].astype(F32)
            width = total.shape[1]
            span = slice(j * width, (j + 1) * width)
            emit(span, (base(span).astype(F32) + total).astype(BF16))

    for copy in locals_ + [own_tok]:
        copy.wait()
    for copy in share(0, feat):
        copy.start()
    forward(0, z)
    forward(1, z)
    uv[...] = jnp.zeros_like(uv)
    gv[...] = jnp.zeros_like(gv)
    share_wait(0, feat)
    norm(feat, mix_gain)

    def in_block(block):
        for r in range(nr):
            rows = slice(r * seq, (r + 1) * seq)
            uv[rows, :] += jnp.dot(
                normed[block, rows, :], g_in[block], preferred_element_type=F32
            )

    stage_loop(0, in_block, 0, lambda: forward(2, z))

    groups, block_len = mixw.shape[0], mixw.shape[1]
    group_width = uv.shape[1] // 2 // groups

    for r in range(nr):
        def mix_rows(i, _):
            start = pl.multiple_of(i * block_len, block_len)
            rows = pl.ds(pl.multiple_of(r * seq + i * block_len, block_len), block_len)
            for g in range(groups):
                at = g * group_width
                half = groups * group_width
                activated = jax.nn.gelu(uv[rows, half + at : half + at + group_width])
                centred = activated - jnp.mean(activated, axis=1, keepdims=True)
                spread = jnp.mean(centred * centred, axis=1, keepdims=True)
                v_norm = (
                    centred * lax.rsqrt(spread + EPS_LN) * norm_gain[:, at : at + group_width]
                ).astype(BF16)
                mixed = jnp.dot(mixw[g], v_norm, preferred_element_type=F32) + bias[g]
                hidden[r, pl.ds(start, block_len), at : at + group_width] = (
                    jax.nn.gelu(uv[rows, at : at + group_width]) * mixed
                ).astype(BF16)
            return 0

        lax.fori_loop(0, seq // block_len, mix_rows, 0)

    stage_loop(
        1, functools.partial(project, 0, hidden, g_out, part1, got1), 0, lambda: forward(3, z)
    )

    def relay(stage, begin, end):
        def step(i, _):
            arrived(stage, order(i) * 2 + y)
            forward(stage, order(i))
            return 0

        lax.fori_loop(begin, end, step, 0)

    def put_middle(span, value):
        feat2[rep, tp, :, span] = value

    relay(2, 1, nz // 2)
    collect(0, part1, got1, lambda span: tok[:, span], put_middle)
    for copy in share(1, feat2):
        copy.start()
    relay(2, nz // 2, nz)
    share_wait(1, feat2)
    norm(feat2, ffn_gain)

    def up_block(block):
        for r in range(nr):
            gv[r, 8:, :] += jnp.dot(
                normed[block, r * seq : (r + 1) * seq, :],
                g_up[block],
                preferred_element_type=F32,
            )

    def up_step(i, _):
        up_block(order(i) * 2 + y)

        @pl.when(i > 0)
        def _():
            arrived(3, order(i) * 2 + y)
            forward(3, order(i))

        other = order(i) * 2 + 1 - y
        arrived(2, other)
        up_block(other)
        return 0

    lax.fori_loop(0, nz, up_step, 0)

    units = act.shape[2]
    taps_len = taps_g.shape[0]
    chunk = 128 if units % 128 == 0 else units
    for r in range(nr):
        for at in range(0, units, chunk):
            gate = jnp.zeros((seq, chunk), F32)
            value = jnp.zeros((seq, chunk), F32)
            for k in range(taps_len):
                first = 8 - (taps_len - 1) + k
                gate += taps_g[k : k + 1, at : at + chunk] * gv[r, first : first + seq, at : at + chunk]
                value += (
                    taps_v[k : k + 1, at : at + chunk]
                    * gv[r, first : first + seq, units + at : units + at + chunk]
                )
            act[r, :, at : at + chunk] = (jax.nn.gelu(gate) * value).astype(BF16)

    down = functools.partial(project, 1, act, g_dn, part2, got2)

    def down_own(i, _):
        down(order(i) * 2 + y)
        return 0

    def down_other(i, _):
        arrived(3, order(i) * 2 + 1 - y)
        down(order(i) * 2 + 1 - y)
        return 0

    lax.fori_loop(0, nz, down_own, 0)
    lax.fori_loop(0, nz, down_other, 0)

    def put_out(span, value):
        out[:, span] = value

    collect(1, part2, got2, lambda span: feat2[rep, tp, :, span], put_out)

    for turn, slabs in enumerate((feat, feat2)):
        for copy in share(turn, slabs):
            copy.wait_send()

    def drain_pieces(block, _):
        for r in range(nr):
            @pl.when(abroad(block, r))
            def _():
                piece(0, part1, got1, block, r).wait_send()
                piece(1, part2, got2, block, r).wait_send()
        return 0

    lax.fori_loop(0, n, drain_pieces, 0)

    def drain_hops(src, _):
        for stage in range(4):
            hop(stage, src * 2 + y, 2).wait_send()
            for way, used in enumerate(ways(src)):
                @pl.when(used)
                def _():
                    hop(stage, src * 2 + y, way).wait_send()
        return 0

    lax.fori_loop(0, nz, drain_hops, 0)


def on_device(
    tokens,
    mix_gain,
    w_u,
    w_v,
    norm_gain,
    mix_weight,
    mix_bias,
    w_mix_out,
    ffn_gain,
    w_gate,
    w_value,
    taps_gate,
    taps_value,
    w_down,
):
    n, nr, nt = lax.axis_size("fs"), lax.axis_size("rep"), lax.axis_size("tp")
    seq, own_width = tokens.shape
    depth, per = own_width * nt // n, n // nt
    block_len = mix_weight.shape[1]
    lower_mask = jnp.arange(block_len)[:, None] >= jnp.arange(block_len)[None, :]
    mixw = own_half(mix_weight, 0)
    mixw = jnp.where(lower_mask[None], mixw, jnp.zeros_like(mixw))
    w_in = jnp.concatenate((own_half(w_u, 1), own_half(w_v, 1)), 1)
    w_up = jnp.concatenate((own_half(w_gate, 1), own_half(w_value, 1)), 1)
    w_out, w_dn = own_half(w_mix_out, 0), own_half(w_down, 0)
    operands = (
        tokens,
        mix_gain.reshape(n, 1, depth),
        w_in,
        own_half(norm_gain, 0)[None, :],
        mixw,
        own_half(mix_bias, 0)[:, :, None],
        w_out,
        ffn_gain.reshape(n, 1, depth),
        w_up,
        own_half(taps_gate, 1).astype(F32),
        own_half(taps_value, 1).astype(F32),
        w_dn,
    )
    vmem, sem = pltpu.VMEM, pltpu.SemaphoreType.DMA
    others = nr * nt - 1
    return pl.pallas_call(
        functools.partial(layer_kernel, n, nr, nt),
        out_shape=jax.ShapeDtypeStruct((seq, own_width), BF16),
        in_specs=[pl.BlockSpec(memory_space=vmem)] * len(operands),
        out_specs=pl.BlockSpec(memory_space=vmem),
        scratch_shapes=[
            vmem((n,) + w_in.shape, BF16),
            vmem((n,) + w_out.shape, BF16),
            vmem((n,) + w_up.shape, BF16),
            vmem((n,) + w_dn.shape, BF16),
            vmem((nr, nt, seq, own_width), BF16),
            vmem((nr, nt, seq, own_width), BF16),
            vmem((n, nr * seq, depth), BF16),
            vmem((nr * seq, w_in.shape[1]), F32),
            vmem((nr, seq, w_out.shape[0]), BF16),
            vmem((nr, seq + 8, w_up.shape[1]), F32),
            vmem((nr, seq, w_dn.shape[0]), BF16),
            vmem((n, nr, seq, depth), BF16),
            vmem((n, nr, seq, depth), BF16),
            vmem((nr * nt, per, seq, depth), BF16),
            vmem((nr * nt, per, seq, depth), BF16),
            sem((4, 3, n)),
            sem((4, n)),
            sem((5,)),
            sem((2, others)),
            sem((2, others)),
            sem((2, n, nr)),
            sem((2, nr * nt, per)),
        ],
        compiler_params=pltpu.CompilerParams(
            collective_id=0, has_side_effects=True, vmem_limit_bytes=67043328
        ),
    )(*operands)


def solution(mesh):
    placed = (
        P(("rep", "fs"), "tp"),
        P(),
        P("fs", "tp"),
        P("fs", "tp"),
        P("tp"),
        P("tp", None, None),
        P("tp", None),
        P("tp", "fs"),
        P(),
        P("fs", "tp"),
        P("fs", "tp"),
        P(None, "tp"),
        P(None, "tp"),
        P("tp", "fs"),
    )
    return jax.shard_map(
        on_device, mesh=mesh, in_specs=placed, out_specs=P(("rep", "fs"), "tp"), check_vma=False
    )
```

time: 604 us -> 232 us (0.38)
  waiting for transfers between devices: 538 us -> 0 us
  Pallas kernels: 0 us -> 217 us
  matrix products: 40.4 us -> 0 us
  between operations: 13.4 us -> 0.04 us
    all_gather x7 -> x0, waiting for transfers between devices: 510 us -> none  [the longest x1 99.8 us: on_device(): lax.all_gather(w_gate, 'fs', axis=0, tiled=True)]
    pallas_call x0 -> x1, Pallas kernels: none -> 217 us  [on_device(): pl.pallas_call(functools.partial(layer_kernel, n, nr, nt), out_shape=jax....]
    dot_general x6 -> x0, matrix products: 40.4 us -> none  [the longest x2 21.5 us: project_with(): return jnp.dot(operand, weight_piece, preferred_element_type=jnp.float32)]
    psum x1 -> x0, waiting for transfers between devices: 16.2 us -> none  [on_device(): lax.psum(mixer_terms.astype(jnp.bfloat16), 'tp').astype(jnp.float32)]
    reduce_scatter x1 -> x0, waiting for transfers between devices: 7.28 us -> none  [on_device(): lax.psum_scatter(down_terms.astype(jnp.bfloat16), 'tp', scatter_dimension...]
  transfers between devices with their start and end apart: 9 -> 0, of which waited for: 9 -> 0; matrix products, arithmetic and copies ran while one was open for 5% -> 0% of each run, Pallas kernels for 0% -> 0%
where the time goes in v2:
time: 232 us; the launch traced here: 230 us
  Pallas kernels  217 us (94%)
  local copies, waits for them, and re-layouts  8.26 us (4%)
  other arithmetic  4.69 us (2%)
    pallas_call x1, Pallas kernels, on_device(): pl.pallas_call(functools.partial(layer_kernel, n, nr, nt), out_shape=jax....  217 us

profile of v2, /device:TPU:0, one launch (start us, length us, event | category | flops | bytes accessed | tf_op | source)
XLA Modules:
  0.0 230.4 jit_solution(5003898782789863340)
XLA Ops:
  0.0 0.0 copy-start
  0.0 1.4 dynamic_slice.35
  1.4 0.7 fusion
  2.1 1.3 dynamic-slice_convert_fusion
  3.4 1.6 dynamic-slice_select_fusion.mixw
  5.0 0.0 copy-start.3
  5.0 0.0 copy-start.4
  5.0 0.9 copy.15.bias
  5.9 1.7 constant_dynamic-slice_fusion.3.w_out
  7.5 0.0 copy-done
  7.6 0.8 constant_dynamic-slice_fusion.w_dn
  8.3 0.0 copy-done.3
  8.3 0.0 copy-done.4
  8.3 0.0 copy-start.2
  8.4 0.0 copy-start.1
  8.4 0.9 pad_maximum_fusion.1.w_in
  9.3 0.4 copy-done.2
  9.7 0.2 copy-done.1
  9.9 0.1 constant_dynamic-slice_fusion.1
  10.0 0.9 pad_maximum_fusion.w_up
  10.9 217.4 %shard_map.136 = bf16[384,1024]{1,0:T(8,128)(2,1)} custom-call(bf16[384,1024]{1,0:T(8,128)(2,1)} %tok.1, f32[8,1,256]{2,1,0:T(1,128)} %bitcast.6, bf16[256,1024]{1,0:T(8,128)(2,1)} %pad_maximum_fusion.1.w_in, f32[1,512]{1,0:T(1,128)} %bitcast.5, bf16[4,128,128]{2,1,0:T(8,128)(2,1)} %dynamic-slice_select_fusion.mixw, f32[4,128,1]{2,1,0:T(8,128)} %copy.15.bias, ...), custom_call_target="tpu_custom_call" | custom-call | tf_op jit(solution)/shard_map/pallas_call | solution.py:385
  228.3 2.1 copy.17
  (2 shorter events, 0.1 us)
Async XLA Ops:
  0.0 7.6 %copy-start = (bf16[1536,256]{1,0:T(8,128)(2,1)S(1)}, bf16[1536,256]{1,0:T(8,128)(2,1)}, u32[]{:S(2)}) copy-start(bf16[1536,256]{1,0:T(8,128)(2,1)} %param.27) | copy-start | bytes 2359300
  5.0 3.4 %copy-start.3 = (bf16[256,1024]{1,0:T(8,128)(2,1)S(1)}, bf16[256,1024]{1,0:T(8,128)(2,1)}, u32[]{:S(2)}) copy-start(bf16[256,1024]{1,0:T(8,128)(2,1)} %param.17) | copy-start | bytes 1572868
  5.0 3.4 %copy-start.4 = (bf16[256,1024]{1,0:T(8,128)(2,1)S(1)}, bf16[256,1024]{1,0:T(8,128)(2,1)}, u32[]{:S(2)}) copy-start(bf16[256,1024]{1,0:T(8,128)(2,1)} %param.16) | copy-start | bytes 1572868
  8.3 1.3 copy-start.2
  8.4 1.5 copy-start.1

commit v3 on v2

--- a/solution.py
+++ b/solution.py
@@ -195,6 +195,7 @@
         copy.start()
     forward(0, z)
     forward(1, z)
+    forward(2, z)
     uv[...] = jnp.zeros_like(uv)
     gv[...] = jnp.zeros_like(gv)
     share_wait(0, feat)
@@ -207,7 +208,7 @@
                 normed[block, rows, :], g_in[block], preferred_element_type=F32
             )
 
-    stage_loop(0, in_block, 0, lambda: forward(2, z))
+    stage_loop(0, in_block, 0, lambda: forward(3, z))
 
     groups, block_len = mixw.shape[0], mixw.shape[1]
     group_width = uv.shape[1] // 2 // groups
@@ -234,7 +235,7 @@
         lax.fori_loop(0, seq // block_len, mix_rows, 0)
 
     stage_loop(
-        1, functools.partial(project, 0, hidden, g_out, part1, got1), 0, lambda: forward(3, z)
+        1, functools.partial(project, 0, hidden, g_out, part1, got1), 0, lambda: None
     )
 
     def relay(stage, begin, end):

time: 232 us -> 228 us (0.983)
  Pallas kernels: 217 us -> 214 us
    pallas_call x1, Pallas kernels: 217 us -> 214 us  [on_device(): pl.pallas_call(functools.partial(layer_kernel, n, nr, nt), out_shape=jax....]
where the time goes in v3:
time: 228 us; the launch traced here: 227 us
  Pallas kernels  214 us (94%)
  local copies, waits for them, and re-layouts  8.26 us (4%)
  other arithmetic  4.69 us (2%)
    pallas_call x1, Pallas kernels, on_device(): pl.pallas_call(functools.partial(layer_kernel, n, nr, nt), out_shape=jax....  214 us

profile of v3, /device:TPU:0, one launch (start us, length us, event | category | flops | bytes accessed | tf_op | source)
XLA Modules:
  0.0 227.3 jit_solution(5411179548255535654)
XLA Ops:
  0.0 0.0 copy-start
  0.0 1.4 dynamic_slice.35
  1.4 0.7 fusion
  2.1 1.3 dynamic-slice_convert_fusion
  3.4 1.6 dynamic-slice_select_fusion.mixw
  5.0 0.0 copy-start.3
  5.0 0.0 copy-start.4
  5.0 0.9 copy.15.bias
  5.9 1.7 constant_dynamic-slice_fusion.3.w_out
  7.5 0.0 copy-done
  7.6 0.8 constant_dynamic-slice_fusion.w_dn
  8.3 0.0 copy-done.3
  8.3 0.0 copy-done.4
  8.3 0.0 copy-start.2
  8.4 0.0 copy-start.1
  8.4 0.9 pad_maximum_fusion.1.w_in
  9.3 0.4 copy-done.2
  9.7 0.2 copy-done.1
  9.9 0.1 constant_dynamic-slice_fusion.1
  10.0 0.9 pad_maximum_fusion.w_up
  10.9 214.3 %shard_map.136 = bf16[384,1024]{1,0:T(8,128)(2,1)} custom-call(bf16[384,1024]{1,0:T(8,128)(2,1)} %tok.1, f32[8,1,256]{2,1,0:T(1,128)} %bitcast.6, bf16[256,1024]{1,0:T(8,128)(2,1)} %pad_maximum_fusion.1.w_in, f32[1,512]{1,0:T(1,128)} %bitcast.5, bf16[4,128,128]{2,1,0:T(8,128)(2,1)} %dynamic-slice_select_fusion.mixw, f32[4,128,1]{2,1,0:T(8,128)} %copy.15.bias, ...), custom_call_target="tpu_custom_call" | custom-call | tf_op jit(solution)/shard_map/pallas_call | solution.py:386
  225.2 2.1 copy.17
  (2 shorter events, 0.1 us)
Async XLA Ops:
  0.0 7.6 %copy-start = (bf16[1536,256]{1,0:T(8,128)(2,1)S(1)}, bf16[1536,256]{1,0:T(8,128)(2,1)}, u32[]{:S(2)}) copy-start(bf16[1536,256]{1,0:T(8,128)(2,1)} %param.27) | copy-start | bytes 2359300
  5.0 3.4 %copy-start.3 = (bf16[256,1024]{1,0:T(8,128)(2,1)S(1)}, bf16[256,1024]{1,0:T(8,128)(2,1)}, u32[]{:S(2)}) copy-start(bf16[256,1024]{1,0:T(8,128)(2,1)} %param.17) | copy-start | bytes 1572868
  5.0 3.4 %copy-start.4 = (bf16[256,1024]{1,0:T(8,128)(2,1)S(1)}, bf16[256,1024]{1,0:T(8,128)(2,1)}, u32[]{:S(2)}) copy-start(bf16[256,1024]{1,0:T(8,128)(2,1)} %param.16) | copy-start | bytes 1572868
  8.3 1.3 copy-start.2
  8.4 1.5 copy-start.1
